TPU v7x, 128 devices: a whole 4x4x4 slice. The times are simulated.
128 devices in a mesh: sp: 32 (over z, y, core), tp: 4 (over x).
Axes of the slice: x: 4, y: 4, z: 4, core: 2. Of those that a mesh axis runs over, the one named last changes fastest.
Arguments:
- tokens: bfloat16 [8192, 4096], P(('sp', 'tp')), may hold values from -6 to 6, as said below
- query_one: bfloat16 [4096, 1024], P('sp', 'tp'), may hold values from -0.125 to 0.125
- query_two: bfloat16 [4096, 1024], P('sp', 'tp'), may hold values from -0.125 to 0.125
- key_one: bfloat16 [4096, 1024], P('sp', 'tp'), may hold values from -0.125 to 0.125
- key_two: bfloat16 [4096, 1024], P('sp', 'tp'), may hold values from -0.125 to 0.125
- value_weight: bfloat16 [4096, 2048], P('sp', 'tp'), may hold values from -0.09375 to 0.09375
- out_weight: bfloat16 [2048, 4096], P('tp', 'sp'), may hold values from -0.125 to 0.125
- lambdas: float32 [8], P('tp'), may hold values from 0.3 to 0.8
- head_gain: float32 [256], replicated, may hold values from 0.1 to 1.9
Outputs:
- layer_out: bfloat16 [8192, 4096], P(('sp', 'tp'))
Inputs may be any that keep to these rules, and one draw needn't show every extreme that they name: `tokens`: the features' mean changes between 16 equal spans of the sequence.
All inputs are finite; a program needn't handle non-finite values.
Results may differ from a plain program's by a relative error of at most 0.013.
The roundings to bfloat16 on the way count: a program that leaves them out, or rounds other values in their place, can miss the bound.
Values may be sent and summed in bfloat16 or wider, within the bound.
A program may use at most 128 MiB of HBM per device.

v0:
```python
import jax
import jax.numpy as jnp
from jax import lax
from jax.sharding import PartitionSpec as P

QK = 128
V = 256


ROPE_BASE = 500000.0
EPS_NORM = 0.02


def copy_for_each(shard, axis):
    count = lax.axis_size(axis)
    return lax.all_to_all(
        jnp.broadcast_to(shard[None], (count, *shard.shape)), axis, 0, 0, tiled=True
    )


def joined_along(pieces, dim):
    dims = list(pieces.shape[1:])
    dims[dim] *= pieces.shape[0]
    return jnp.moveaxis(pieces, 0, dim).reshape(dims)


def collect(shard, axis, dim):
    pieces = copy_for_each(shard, axis)
    return joined_along(pieces, dim)


def sent_together(arrays, axis, dim, along):
    widths = [a.shape[along] for a in arrays]
    both = jnp.concatenate(arrays, axis=along)
    result = lax.all_gather(both, axis, axis=dim, tiled=True)
    return tuple(jnp.split(result, [sum(widths[:k]) for k in range(1, len(widths))], axis=along))


def cut_along(shard, dim, count):
    before, after = (shard.shape[:dim], shard.shape[dim + 1 :])
    return jnp.moveaxis(shard.reshape(*before, count, -1, *after), dim, 0)


def sum_at_owner(shard, axis, dim):
    pieces = cut_along(shard, dim, lax.axis_size(axis))
    arrived = lax.all_to_all(pieces, axis, split_axis=0, concat_axis=0, tiled=True)
    return arrived.astype(jnp.float32).sum(axis=0)


def rotate(values, positions):
    half_dim = values.shape[-1] // 2
    inverse = 1.0 / ROPE_BASE ** (
        jnp.arange(0, 2 * half_dim, 2, dtype=jnp.float32) / (2 * half_dim)
    )
    angles = positions.astype(jnp.float32)[:, None] * inverse[None, :]
    cos_part = jnp.cos(angles)[:, None, :]
    sin_part = jnp.sin(angles)[:, None, :]
    first_half = values[..., :half_dim]
    second_half = values[..., half_dim:]
    return jnp.concatenate(
        [
            first_half * cos_part - second_half * sin_part,
            second_half * cos_part + first_half * sin_part,
        ],
        axis=-1,
    )


def unchanged(carried):
    return carried


def on_device(
    tokens, query_one, query_two, key_one, key_two, value_weight, out_weight, lambdas, head_gain
):
    tp_count = lax.axis_size("tp")
    sp_index = lax.axis_index("sp")
    own_rows = tokens.shape[0]
    local_len = own_rows * tp_count
    half_len = local_len // 2
    heads_here = lambdas.shape[0]
    gathered = collect(tokens, "tp", 0)
    row_ids = jnp.arange(local_len, dtype=jnp.int32)
    query_pos = sp_index * local_len + row_ids
    pieces = sent_together((query_one, query_two, key_one, key_two, value_weight), "sp", 0, 1)
    projected = tuple(
        (
            jnp.dot(gathered, weight_piece, preferred_element_type=jnp.float32)
            for weight_piece in pieces
        )
    )

    def turned(product):
        return rotate(product.reshape(local_len, heads_here, QK), query_pos).astype(jnp.bfloat16)

    q_one = turned(projected[0])
    q_two = turned(projected[1])
    k_one = turned(projected[2]).reshape(local_len, heads_here * QK)
    k_two = turned(projected[3]).reshape(local_len, heads_here * QK)
    values = projected[4].astype(jnp.bfloat16)
    scale = QK ** (-0.5)
    pieces = sent_together((k_one, k_two, values), "sp", 0, 1)
    key_count = pieces[0].shape[0]
    global_ids = jnp.arange(key_count, dtype=jnp.int32)
    shard_ids = global_ids // local_len
    within = global_ids % local_len
    key_pos = shard_ids * local_len + within
    key_sets = (
        pieces[0].reshape(key_count, heads_here, QK),
        pieces[1].reshape(key_count, heads_here, QK),
    )
    value_rows = pieces[2].reshape(key_count, heads_here, V)
    row_tops = jnp.full((2, heads_here, local_len), -1e30, jnp.float32)
    totals = jnp.zeros((2, heads_here, local_len), jnp.float32)
    accums = jnp.zeros((2, heads_here, local_len, V), jnp.float32)
    new_parts = []
    for segment in range(2):
        low_row = segment * half_len
        seg_pos = query_pos[low_row : low_row + half_len]
        queries = (q_one[low_row : low_row + half_len], q_two[low_row : low_row + half_len])
        carried = (
            row_tops[:, :, low_row : low_row + half_len],
            totals[:, :, low_row : low_row + half_len],
            accums[:, :, low_row : low_row + half_len],
        )

        def update(carried, queries=queries, seg_pos=seg_pos):
            allowed = key_pos[None, :] <= seg_pos[:, None]
            out_tops, out_totals, out_accums = ([], [], [])
            for map_index in range(2):
                scores = (
                    jnp.einsum(
                        "qhd,khd->hqk",
                        queries[map_index],
                        key_sets[map_index],
                        preferred_element_type=jnp.float32,
                    )
                    * scale
                )
                masked = jnp.where(allowed[None], scores, -1e30)
                old_top = carried[0][map_index]
                new_top = jnp.maximum(old_top, jnp.max(masked, axis=-1))
                exp_weights = jnp.where(allowed[None], jnp.exp(scores - new_top[..., None]), 0.0)
                new_total = jnp.sum(exp_weights, axis=-1)
                new_accum = jnp.einsum(
                    "hqk,khv->hqv",
                    exp_weights.astype(jnp.bfloat16),
                    value_rows,
                    preferred_element_type=jnp.float32,
                )
                out_tops.append(new_top)
                out_totals.append(new_total)
                out_accums.append(new_accum)
            return (jnp.stack(out_tops), jnp.stack(out_totals), jnp.stack(out_accums))

        needed = jnp.min(key_pos) <= jnp.max(seg_pos)
        new_parts.append(lax.cond(needed, update, unchanged, carried))
    row_tops, totals, accums = tuple(
        (
            jnp.concatenate([new_part[member] for new_part in new_parts], axis=2)
            for member in range(3)
        )
    )
    map_outputs = accums / totals[..., None]
    mixed_out = map_outputs[0] - lambdas[:, None, None] * map_outputs[1]
    scaled = (
        mixed_out
        * lax.rsqrt(jnp.mean(mixed_out * mixed_out, axis=-1, keepdims=True) + EPS_NORM)
        * head_gain
    )
    attended = scaled.astype(jnp.bfloat16)
    weight_piece = lax.all_gather(out_weight, "sp", axis=1, tiled=True)
    shaped = weight_piece.reshape(heads_here, V, weight_piece.shape[1])
    partial_terms = jnp.einsum("hqv,hvd->qd", attended, shaped, preferred_element_type=jnp.float32)
    summed = sum_at_owner(partial_terms.astype(jnp.bfloat16), "tp", 0).astype(jnp.bfloat16)
    return summed


def solution(mesh):
    in_specs = (
        P(("sp", "tp"), None),
        P("sp", "tp"),
        P("sp", "tp"),
        P("sp", "tp"),
        P("sp", "tp"),
        P("sp", "tp"),
        P("tp", "sp"),
        P("tp"),
        P(),
    )
    out_specs = P(("sp", "tp"), None)
    return jax.shard_map(
        on_device, mesh=mesh, in_specs=in_specs, out_specs=out_specs, check_vma=False
    )
```

profile of v0, /device:TPU:1, one launch (start us, length us, event | category | flops | bytes accessed | tf_op | source)
XLA Modules:
  0.0 316.2 jit_solution(6942808003568781674)
XLA Ops:
  11.6 2.7 broadcast_in_dim.90
  14.3 4.8 %all-to-all-start = ((bf16[4,64,4096]{2,1,0:T(8,128)(2,1)}), bf16[4,64,4096]{2,1,0:T(8,128)(2,1)S(1)}, u32[]{:S(2)}, u32[]{:S(2)}) async-start(bf16[4,64,4096]{2,1,0:T(8,128)(2,1)} %broadcast_in_dim.90), calls=%async_computation | async-start | bytes 4194304 | tf_op jit(solution)/shard_map/all_to_all | solution.py:16
  20.4 24.2 %all-to-all-done = bf16[4,64,4096]{2,1,0:T(8,128)(2,1)S(1)} async-done(((bf16[4,64,4096]{2,1,0:T(8,128)(2,1)}), bf16[4,64,4096]{2,1,0:T(8,128)(2,1)S(1)}, u32[]{:S(2)}, u32[]{:S(2)}) %all-to-all-start) | async-done | bytes 2097184 | tf_op jit(solution)/shard_map/all_to_all | solution.py:16
  44.6 33.7 %all-gather.4.cloned.1.call-done = bf16[4096,1536]{1,0:T(8,128)(2,1)} async-done(((bf16[128,1536]{1,0:T(8,128)(2,1)}), bf16[4096,1536]{1,0:T(8,128)(2,1)}) %all-gather.4.cloned.1.call-update) | async-done | bytes 12582928 | tf_op jit(solution)/shard_map/all_gather | solution.py:35
  81.0 2.3 fusion.55
  83.6 2.3 fusion.53
  97.8 3.5 %fusion.62 = bf16[256,512]{0,1:T(8,128)(2,1)S(1)} fusion(bf16[256,4096]{1,0:T(8,128)(2,1)S(1)} %bitcast.73, bf16[4096,1536]{1,0:T(8,128)(2,1)} %all-gather.4.cloned.1.call-done), kind=kOutput, calls=%fused_computation.71 | convolution fusion | flops 1073872896 | bytes 6553600 | tf_op jit(solution)/shard_map/dot_general | solution.py:88
  107.0 74.9 %all-gather.6.cloned.1.call-done = bf16[8192,1024]{0,1:T(8,128)(2,1)} async-done(((bf16[256,1024]{0,1:T(8,128)(2,1)}), bf16[8192,1024]{0,1:T(8,128)(2,1)}) %all-gather.6.cloned.1.call-update) | async-done | bytes 16777232 | tf_op jit(solution)/shard_map/all_gather | solution.py:35
  181.9 7.6 %split.39 = bf16[8192,512]{0,1:T(8,128)(2,1)} slice(bf16[8192,1024]{0,1:T(8,128)(2,1)} %all-gather.6.cloned.1.call-done), slice={[0:8192], [512:1024]} | slice | bytes 16777216 | tf_op jit(solution)/shard_map/split | solution.py:36
  189.5 5.2 %fusion.84 = (bf16[8192,256]{0,1:T(8,128)(2,1)}, bf16[8192,256]{0,1:T(8,128)(2,1)S(1)}) fusion(bf16[8192,1024]{0,1:T(8,128)(2,1)} %all-gather.6.cloned.1.call-done), kind=kLoop, calls=%fused_computation.123 | loop fusion | bytes 16777216 | tf_op jit(solution)/shard_map/split | solution.py:36
  196.7 38.6 %conditional.2 = (f32[2,2,128]{2,1,0:T(2,128)S(1)}, f32[2,2,128,256]{3,2,1,0:T(8,128)S(1)}) conditional(s32[]{:T(128)} %convert_element_type.57, () %tuple.21, (s32[8192]{0:T(1024)S(1)}, s32[128]{0:T(128)S(1)}, bf16[256,2,128]{2,0,1:T(8,128)(2,1)S(1)}, bf16[8192,2,128]{0,2,1:T(8,128)(2,1)S(1)}, bf16[256,2,128]{2,0,1:T(8,128)(2,1)S(1)}, ...), branch_computations={%region_2.3_spmd, %region_3.8_spmd} | conditional | flops 3260153856 | bytes 117097000 | solution.py:157
  197.4 2.5 select_reduce_fusion.1
  199.9 12.5 %fusion.1 = (f32[2,128]{1,0:T(2,128)S(1)}, f32[2,128]{1,0:T(2,128)S(1)}, f32[2,128,8192]{2,1,0:T(8,128)}) fusion(f32[2,128,8192]{2,1,0:T(8,128)S(1)} %get-tuple-element.80, f32[2,128]{1,0:T(2,128)S(1)} %broadcast_maximum_fusion.1, pred[128,8192]{1,0:T(8,128)(4,1)S(1)} %broadcast_compare_fusion, bf16[8192,2,128]{0,2,1:T(8,128)(2,1)} %get-tuple-element.64, ...), kind=kOutput, calls=%fused_computation.7 | convolution fusion | flops 549453312 | bytes 22088704 | tf_op jit(solution)/shard_map/cond/branch_1_fun/qhd,khd->hqk/dot_general | solution.py:132
  212.4 9.1 %fusion.17 = f32[1,2,128,256]{3,2,1,0:T(8,128)S(1)} fusion(bf16[8192,2,256]{0,2,1:T(8,128)(2,1)} %get-tuple-element.65, f32[2,128,8192]{2,1,0:T(8,128)} %get-tuple-element.81, f32[2,128]{1,0:T(2,128)S(1)} %broadcast_maximum_fusion, pred[128,8192]{1,0:T(8,128)(4,1)S(1)} %broadcast_compare_fusion), kind=kOutput, calls=%fused_computation.20 | convolution fusion | flops 1080033280 | bytes 18088960 | tf_op jit(solution)/shard_map/cond/branch_1_fun/hqk,khv->hqv/dot_general | solution.py:145
  221.5 9.0 %fusion.14 = f32[1,2,128,256]{3,2,1,0:T(8,128)S(1)} fusion(bf16[8192,2,256]{0,2,1:T(8,128)(2,1)} %get-tuple-element.65, f32[2,128,8192]{2,1,0:T(8,128)} %copy-done.1, f32[2,128]{1,0:T(2,128)S(1)} %broadcast_maximum_fusion.1, pred[128,8192]{1,0:T(8,128)(4,1)S(1)} %broadcast_compare_fusion), kind=kOutput, calls=%fused_computation.19 | convolution fusion | flops 1080033280 | bytes 18088960 | tf_op jit(solution)/shard_map/cond/branch_1_fun/hqk,khv->hqv/dot_general | solution.py:145
  230.6 4.5 %fusion.3 = f32[2,128]{1,0:T(2,128)S(1)} fusion(f32[2,128,8192]{2,1,0:T(8,128)} %get-tuple-element.81, f32[2,128]{1,0:T(2,128)S(1)} %broadcast_maximum_fusion, pred[128,8192]{1,0:T(8,128)(4,1)S(1)} %broadcast_compare_fusion), kind=kLoop, calls=%fused_computation.9 | loop fusion | flops 6291200 | bytes 9439232 | tf_op jit(solution)/shard_map/cond/branch_1_fun/reduce_sum | solution.py:144
  235.3 39.8 %conditional.3 = (f32[2,2,128]{2,1,0:T(2,128)S(1)}, f32[2,2,128,256]{3,2,1,0:T(8,128)S(1)}) conditional(s32[]{:T(128)} %convert_element_type.63, () %tuple.23, (s32[8192]{0:T(1024)S(1)}, s32[128]{0:T(128)S(1)}, bf16[256,2,128]{2,0,1:T(8,128)(2,1)S(1)}, bf16[8192,2,128]{0,2,1:T(8,128)(2,1)}, bf16[256,2,128]{2,0,1:T(8,128)(2,1)S(1)}, ...), branch_computations={%region_9.10_spmd, %region_10.15_spmd} | conditional | flops 3260153856 | bytes 117097000 | solution.py:157
  236.0 4.6 %select_reduce_fusion.3 = (f32[2,128]{1,0:T(2,128)S(1)}, f32[2,128,8192]{2,1,0:T(8,128)S(1)}) fusion(pred[128,8192]{1,0:T(8,128)(4,1)S(1)} %broadcast_compare_fusion.1, bf16[8192,2,128]{0,2,1:T(8,128)(2,1)} %get-tuple-element.69, bf16[256,2,128]{2,0,1:T(8,128)(2,1)S(1)} %get-tuple-element.46), kind=kOutput, calls=%fused_computation.34 | convolution fusion | flops 543162112 | bytes 13698048 | tf_op jit(solution)/shard_map/cond/branch_1_fun/qhd,khd->hqk/dot_general | solution.py:132
  240.6 12.5 %fusion.25 = (f32[2,128]{1,0:T(2,128)S(1)}, f32[2,128]{1,0:T(2,128)S(1)}, f32[2,128,8192]{2,1,0:T(8,128)}) fusion(f32[2,128,8192]{2,1,0:T(8,128)S(1)} %get-tuple-element.83, f32[2,128]{1,0:T(2,128)S(1)} %broadcast_maximum_fusion.3, pred[128,8192]{1,0:T(8,128)(4,1)S(1)} %broadcast_compare_fusion.1, bf16[8192,2,128]{0,2,1:T(8,128)(2,1)} %get-tuple-element.71, ...), kind=kOutput, calls=%fused_computation.36 | convolution fusion | flops 549453312 | bytes 22088704 | tf_op jit(solution)/shard_map/cond/branch_1_fun/qhd,khd->hqk/dot_general | solution.py:132
  253.1 8.7 %fusion.41 = f32[1,2,128,256]{3,2,1,0:T(8,128)S(1)} fusion(bf16[8192,2,256]{0,2,1:T(8,128)(2,1)} %get-tuple-element.72, f32[2,128,8192]{2,1,0:T(8,128)} %get-tuple-element.84, f32[2,128]{1,0:T(2,128)S(1)} %broadcast_maximum_fusion.2, pred[128,8192]{1,0:T(8,128)(4,1)S(1)} %broadcast_compare_fusion.1), kind=kOutput, calls=%fused_computation.49 | convolution fusion | flops 1080033280 | bytes 18088960 | tf_op jit(solution)/shard_map/cond/branch_1_fun/hqk,khv->hqv/dot_general | solution.py:145
  261.8 8.7 %fusion.38 = f32[1,2,128,256]{3,2,1,0:T(8,128)S(1)} fusion(bf16[8192,2,256]{0,2,1:T(8,128)(2,1)} %get-tuple-element.72, f32[2,128,8192]{2,1,0:T(8,128)} %copy-done.2, f32[2,128]{1,0:T(2,128)S(1)} %broadcast_maximum_fusion.3, pred[128,8192]{1,0:T(8,128)(4,1)S(1)} %broadcast_compare_fusion.1), kind=kOutput, calls=%fused_computation.48 | convolution fusion | flops 1080033280 | bytes 18088960 | tf_op jit(solution)/shard_map/cond/branch_1_fun/hqk,khv->hqv/dot_general | solution.py:145
  270.6 4.5 %fusion.27 = f32[2,128]{1,0:T(2,128)S(1)} fusion(f32[2,128,8192]{2,1,0:T(8,128)} %get-tuple-element.84, f32[2,128]{1,0:T(2,128)S(1)} %broadcast_maximum_fusion.2, pred[128,8192]{1,0:T(8,128)(4,1)S(1)} %broadcast_compare_fusion.1), kind=kLoop, calls=%fused_computation.38 | loop fusion | flops 6291200 | bytes 9439232 | tf_op jit(solution)/shard_map/cond/branch_1_fun/reduce_sum | solution.py:144
  275.6 3.5 %fusion.48 = bf16[256,4096]{1,0:T(8,128)(2,1)S(1)} fusion(bf16[2,256,4096]{2,1,0:T(8,128)(2,1)} %bitcast.85, f32[2,2,256,256]{3,2,1,0:T(8,128)S(1)} %maximum_divide_fusion, f32[256]{0:T(256)S(1)} %copy-done.8, f32[2,256]{1,0:T(2,128)S(1)} %add_rsqrt_fusion, f32[2]{0:T(128)S(1)} %copy-done.7), kind=kOutput, calls=%fused_computation.59 | convolution fusion | flops 1075445760 | bytes 7343112 | tf_op jit(solution)/shard_map/hqv,hvd->qd/dot_general | solution.py:174
  279.1 29.3 %all_to_all.10 = bf16[4,64,4096]{2,1,0:T(8,128)(2,1)S(1)} all-to-all(bf16[4,64,4096]{2,1,0:T(8,128)(2,1)S(1)} %bitcast.74), channel_id=1, replica_groups=mesh['sp'=32,'tp'=4] {'tp'}, dimensions={0} | all-to-all | bytes 4194304 | tf_op jit(solution)/shard_map/all_to_all | solution.py:46
  (73 shorter events, 29.3 us)
Async XLA Ops:
  6.5 71.8 %all-gather.4.cloned.1.call-start = ((), (), s32[]{:S(2)}) async-start(), calls=%async_computation.2 | async-start | bytes 12976128 | tf_op jit(solution)/shard_map/all_gather | solution.py:35
  10.8 0.7 copy-start.3
  14.3 30.3 %all-to-all-start = ((bf16[4,64,4096]{2,1,0:T(8,128)(2,1)}), bf16[4,64,4096]{2,1,0:T(8,128)(2,1)S(1)}, u32[]{:S(2)}, u32[]{:S(2)}) async-start(bf16[4,64,4096]{2,1,0:T(8,128)(2,1)} %broadcast_in_dim.90), calls=%async_computation | async-start | bytes 4194304 | tf_op jit(solution)/shard_map/all_to_all | solution.py:16
  19.1 162.8 %all-gather.6.cloned.1.call-start = ((), (), s32[]{:S(2)}) async-start(), calls=%async_computation.3 | async-start | bytes 17301504 | tf_op jit(solution)/shard_map/all_gather | solution.py:35
  96.4 10.4 %copy-start.5 = (bf16[256,2,64]{2,0,1:T(8,128)(2,1)S(1)}, bf16[256,2,64]{2,0,1:T(8,128)(2,1)}, u32[]{:S(2)}) copy-start(bf16[256,2,64]{2,0,1:T(8,128)(2,1)} %get-tuple-element.87) | copy-start | bytes 196612
  96.4 10.4 %copy-start.6 = (bf16[256,2,64]{2,0,1:T(8,128)(2,1)S(1)}, bf16[256,2,64]{2,0,1:T(8,128)(2,1)}, u32[]{:S(2)}) copy-start(bf16[256,2,64]{2,0,1:T(8,128)(2,1)} %get-tuple-element.88) | copy-start | bytes 196612
  96.4 10.5 %copy-start.4 = (bf16[256,2,64]{2,0,1:T(8,128)(2,1)S(1)}, bf16[256,2,64]{2,0,1:T(8,128)(2,1)}, u32[]{:S(2)}) copy-start(bf16[256,2,64]{2,0,1:T(8,128)(2,1)} %get-tuple-element.100) | copy-start | bytes 196612
  102.2 173.5 %all-gather.8.cloned.1.call-start = ((), (), s32[]{:S(2)}) async-start(), calls=%async_computation.4 | async-start | bytes 4325376 | tf_op jit(solution)/shard_map/all_gather | solution.py:172
  194.7 2.0 copy-start
  199.9 12.5 %copy-start.1 = (f32[2,128,8192]{2,1,0:T(8,128)}, f32[2,128,8192]{2,1,0:T(8,128)S(1)}, u32[]{:S(2)}) copy-start(f32[2,128,8192]{2,1,0:T(8,128)S(1)} %get-tuple-element.80) | copy-start | bytes 25165828 | tf_op jit(solution)/shard_map/cond
  235.3 40.1 %copy-start.7 = (f32[2]{0:T(128)S(1)}, f32[2]{0:T(128)}, u32[]{:S(2)}) copy-start(f32[2]{0:T(128)} %param.20) | copy-start | bytes 28
  235.3 40.3 %copy-start.8 = (f32[256]{0:T(256)S(1)}, f32[256]{0:T(256)}, u32[]{:S(2)}) copy-start(f32[256]{0:T(256)} %param.21) | copy-start | bytes 3076
  240.6 12.5 %copy-start.2 = (f32[2,128,8192]{2,1,0:T(8,128)}, f32[2,128,8192]{2,1,0:T(8,128)S(1)}, u32[]{:S(2)}) copy-start(f32[2,128,8192]{2,1,0:T(8,128)S(1)} %get-tuple-element.83) | copy-start | bytes 25165828 | tf_op jit(solution)/shard_map/cond
Sparse Core Ops, SparseCore 0:
  11.7 66.5 all-gather.3
  102.3 79.5 all-gather.5
  184.1 48.8 all-gather.7
where the time goes:
time: 318 us; the launch traced here: 316 us
  waiting for transfers between devices  134 us (42%)
  matrix products  83.9 us (26%)
  blocking collectives  29.3 us (9%)
  local copies, waits for them, and re-layouts  29.1 us (9%)
  other arithmetic  19.2 us (6%)
  between operations  15.8 us (5%)
  starting transfers between devices  4.88 us (2%)
    all_gather x2, waiting for transfers between devices, sent_together(): result = lax.all_gather(both, axis, axis=dim, tiled=True)  109 us
    dot_general x4, matrix products, update(): jnp.einsum('hqk,khv->hqv', exp_weights.astype(jnp.bfloat16), value_rows,...  35.5 us
    dot_general x4, matrix products, update(): jnp.einsum('qhd,khd->hqk', queries[map_index], key_sets[map_index], prefe...  32.1 us
    all_to_all x1, blocking collectives, sum_at_owner(): lax.all_to_all(pieces, axis, split_axis=0, concat_axis=0, tiled=True)  29.3 us
    all_to_all x1, waiting for transfers between devices, copy_for_each(): lax.all_to_all(jnp.broadcast_to(shard[None], (count, *shard.shape)), axis...  24.2 us
    dot_general x5, matrix products, on_device(): jnp.dot(gathered, weight_piece, preferred_element_type=jnp.float32)  12.9 us
    split x2, local copies, waits for them, and re-layouts, sent_together(): jnp.split(result, [sum(widths[:k]) for k in range(1, len(widths))], axis=...  12.8 us
    unnamed x26, local copies, waits for them, and re-layouts  11.1 us
  transfers between devices with their start and end apart: 4, of which 3 were waited for; matrix products, arithmetic and copies ran while one was open for 31% of the time, Pallas kernels for 0%

commit v1 on v0

v1 whole, which is shorter than its diff:
```python
import functools

import jax
import jax.numpy as jnp
from jax import lax
from jax.experimental import pallas as pl
from jax.experimental.pallas import tpu as pltpu
from jax.sharding import Mesh, PartitionSpec as P

QK = 128
V = 256
ROPE_BASE = 500000.0
EPS_NORM = 0.02
ROWS = 512
LOG2E = 1.4426950408889634


def rope_tables(positions):
    half = QK // 2
    inverse = 1.0 / ROPE_BASE ** (jnp.arange(0, QK, 2, dtype=jnp.float32) / QK)
    angles = positions.astype(jnp.float32)[:, None] * inverse[None, :]
    c, s = jnp.cos(angles), jnp.sin(angles)
    return jnp.concatenate([c, c], axis=1), jnp.concatenate([-s, s], axis=1)


def turned(x, cos, sin):
    half = QK // 2
    swapped = jnp.concatenate([x[:, half:], x[:, :half]], axis=1)
    return (x * cos + swapped * sin).astype(jnp.bfloat16)


def flash_kernel(n_chips, q1_ref, q2_ref, k1_ref, k2_ref, v_ref, lam_ref, gain_ref, out_ref, acc, top, tot):
    chip = lax.axis_index("z") * 4 + lax.axis_index("y")
    scale = QK ** (-0.5)
    qs = (q1_ref, q2_ref)
    ks = (k1_ref, k2_ref)
    for a in range(2):
        top[a] = jnp.full((ROWS, 128), -1e30, jnp.float32)
        tot[a] = jnp.zeros((ROWS, 128), jnp.float32)
        acc[a] = jnp.zeros((ROWS, V), jnp.float32)

    def block(j, diagonal):
        start = pl.multiple_of(j * ROWS, ROWS)
        v = v_ref[pl.ds(start, ROWS), :]
        for a in range(2):
            s = lax.dot_general(
                qs[a][...], ks[a][pl.ds(start, ROWS), :], (((1,), (1,)), ((), ())),
                preferred_element_type=jnp.float32,
            ) * scale
            if diagonal:
                rows = lax.broadcasted_iota(jnp.int32, s.shape, 0)
                cols = lax.broadcasted_iota(jnp.int32, s.shape, 1)
                s = jnp.where(cols <= rows, s, -1e30)
            old = top[a][:, :1]
            new = jnp.maximum(old, jnp.max(s, axis=1, keepdims=True))
            e = jnp.exp(s - new)
            fade = jnp.exp(old - new)
            tot[a] = tot[a] * fade + jnp.sum(e, axis=1, keepdims=True)
            acc[a] = acc[a] * fade + lax.dot_general(
                e.astype(jnp.bfloat16), v, (((1,), (0,)), ((), ())),
                preferred_element_type=jnp.float32,
            )
            top[a] = jnp.broadcast_to(new, (ROWS, 128))

    block(chip, True)

    @pl.loop(0, chip)
    def _(j):
        block(j, False)

    o1 = acc[0] / tot[0][:, :1]
    o2 = acc[1] / tot[1][:, :1]
    mixed = o1 - lam_ref[0] * o2
    norm = lax.rsqrt(jnp.mean(mixed * mixed, axis=1, keepdims=True) + EPS_NORM)
    out_ref[...] = (mixed * norm * gain_ref[...]).astype(jnp.bfloat16)


def flash(q1, q2, k1, k2, v, lam, gain):
    vm = pl.BlockSpec(memory_space=pltpu.VMEM)
    return pl.pallas_call(
        functools.partial(flash_kernel, 16),
        out_shape=jax.ShapeDtypeStruct((ROWS, V), jnp.bfloat16),
        in_specs=[vm] * 5 + [pl.BlockSpec(memory_space=pltpu.SMEM), vm],
        out_specs=vm,
        scratch_shapes=[
            pltpu.VMEM((2, ROWS, V), jnp.float32),
            pltpu.VMEM((2, ROWS, 128), jnp.float32),
            pltpu.VMEM((2, ROWS, 128), jnp.float32),
        ],
        compiler_params=pltpu.CompilerParams(vmem_limit_bytes=60 * 1024 * 1024),
        cost_estimate=pl.CostEstimate(flops=6 * 10**9, bytes_accessed=10**7, transcendentals=10**7),
    )(q1, q2, k1, k2, v, lam, gain)


def on_device(tokens, query_one, query_two, key_one, key_two, value_weight, out_weight, lambdas, head_gain):
    core = lax.axis_index("core")
    chip = lax.axis_index("z") * 4 + lax.axis_index("y")
    rows = lax.all_gather(tokens, ("core", "x"), axis=0, tiled=True)
    by_head = [w.reshape(128, 2, -1) for w in (query_one, query_two, key_one, key_two, value_weight)]
    both = jnp.concatenate(by_head, axis=2)
    mine = lax.all_to_all(both, "core", split_axis=1, concat_axis=0, tiled=True).reshape(256, 768)
    weights = lax.all_gather(mine, ("z", "y"), axis=0, tiled=True)
    projected = jnp.dot(rows, weights, preferred_element_type=jnp.float32)
    cos, sin = rope_tables(chip * ROWS + jnp.arange(ROWS, dtype=jnp.int32))
    q1, q2, k1, k2 = [turned(projected[:, i * QK : (i + 1) * QK], cos, sin) for i in range(4)]
    v = projected[:, 4 * QK :].astype(jnp.bfloat16)
    kv = lax.all_gather(jnp.concatenate([k1, k2, v], axis=1), ("z", "y"), axis=0, tiled=True)
    k1, k2, v = kv[:, :QK], kv[:, QK : 2 * QK], kv[:, 2 * QK :]
    lam = lax.dynamic_slice(lambdas, (core,), (1,))
    attended = flash(q1, q2, k1, k2, v, lam, head_gain[None])
    heads = lax.all_gather(attended, "core", axis=1, tiled=True)
    columns = lax.all_gather(out_weight, ("z", "y"), axis=1, tiled=True)
    part = jnp.dot(heads, columns, preferred_element_type=jnp.float32).astype(jnp.bfloat16)
    part = part.reshape(2, 4, 64, 2048)
    got = lax.all_to_all(part, "x", split_axis=1, concat_axis=1, tiled=True)
    summed = got.astype(jnp.float32).sum(axis=1).astype(jnp.bfloat16)
    both_cores = lax.all_to_all(summed[:, :, None], "core", split_axis=0, concat_axis=2, tiled=True)
    out = both_cores.reshape(64, 2, 16, 128)
    return jnp.swapaxes(out, 1, 2).reshape(64, 4096)


def solution(mesh):
    fine = Mesh(mesh.devices.reshape(4, 4, 2, 4), ("z", "y", "core", "x"))
    sp = ("z", "y", "core")
    in_specs = (
        P((*sp, "x"), None),
        P(sp, "x"),
        P(sp, "x"),
        P(sp, "x"),
        P(sp, "x"),
        P(sp, "x"),
        P("x", sp),
        P("x"),
        P(),
    )
    return jax.shard_map(on_device, mesh=fine, in_specs=in_specs, out_specs=P((*sp, "x"), None), check_vma=False)
```

time: 318 us -> 283 us (0.89)
  matrix products: 83.9 us -> 9.88 us
  waiting for transfers between devices: 134 us -> 188 us
  other arithmetic: 19.2 us -> 3.68 us
  blocking collectives: 29.3 us -> 42.8 us
  local copies, waits for them, and re-layouts: 29.1 us -> 17.3 us
  Pallas kernels: 0 us -> 6.99 us
  starting transfers between devices: 4.88 us -> 0.12 us
    all_gather x3 -> x4, waiting for transfers between devices: 109 us -> 187 us  [the longest x1 69.4 us: on_device(): lax.all_gather(jnp.concatenate([k1, k2, v], axis=1), ('z', 'y'), axis=0,...]
    dot_general x14 -> x2, matrix products: 83.9 us -> 9.88 us  [the longest x1 7.04 us: on_device(): projected = jnp.dot(rows, weights, preferred_element_type=jnp.float32)]
    all_to_all x1 -> x0, waiting for transfers between devices: 24.2 us -> none  [copy_for_each(): lax.all_to_all(jnp.broadcast_to(shard[None], (count, *shard.shape)), axis...]
    split x2 -> x0, local copies, waits for them, and re-layouts: 12.8 us -> none  [sent_together(): jnp.split(result, [sum(widths[:k]) for k in range(1, len(widths))], axis=...]
    all_to_all x1 -> x3, blocking collectives: 29.3 us -> 39.9 us  [the longest x1 27.6 us: on_device(): got = lax.all_to_all(part, 'x', split_axis=1, concat_axis=1, tiled=True)]
    reduce_sum x4 -> x1, other arithmetic: 10.5 us -> 0.43 us  [on_device(): summed = got.astype(jnp.float32).sum(axis=1).astype(jnp.bfloat16)]
    pallas_call x0 -> x1, Pallas kernels: none -> 6.99 us  [flash(): pl.pallas_call(functools.partial(flash_kernel, 16), out_shape=jax.ShapeDt...]
    slice x4, local copies, waits for them, and re-layouts: 1.39 us -> 7.35 us  [the longest x2 6.98 us: on_device(): k1, k2, v = (kv[:, :QK], kv[:, QK:2 * QK], kv[:, 2 * QK:])]
  transfers between devices with their start and end apart: 4 -> 4, of which waited for: 3 -> 4; matrix products, arithmetic and copies ran while one was open for 31% -> 5% of each run, Pallas kernels for 0% -> 2%
where the time goes in v1:
time: 283 us; the launch traced here: 282 us
  waiting for transfers between devices  188 us (66%)
  blocking collectives  42.8 us (15%)
  local copies, waits for them, and re-layouts  17.3 us (6%)
  between operations  13.3 us (5%)
  matrix products  9.88 us (3%)
  Pallas kernels  6.99 us (2%)
  other arithmetic  3.68 us (1%)
    all_gather x1, waiting for transfers between devices, on_device(): lax.all_gather(jnp.concatenate([k1, k2, v], axis=1), ('z', 'y'), axis=0,...  69.4 us
    all_gather x1, waiting for transfers between devices, on_device(): weights = lax.all_gather(mine, ('z', 'y'), axis=0, tiled=True)  63 us
    all_gather x1, waiting for transfers between devices, on_device(): columns = lax.all_gather(out_weight, ('z', 'y'), axis=1, tiled=True)  29 us
    all_to_all x1, blocking collectives, on_device(): got = lax.all_to_all(part, 'x', split_axis=1, concat_axis=1, tiled=True)  27.6 us
    all_gather x1, waiting for transfers between devices, on_device(): rows = lax.all_gather(tokens, ('core', 'x'), axis=0, tiled=True)  25.3 us
    all_to_all x1, blocking collectives, on_device(): lax.all_to_all(summed[:, :, None], 'core', split_axis=0, concat_axis=2, t...  7.19 us
    dot_general x1, matrix products, on_device(): projected = jnp.dot(rows, weights, preferred_element_type=jnp.float32)  7.04 us
    pallas_call x1, Pallas kernels, flash(): pl.pallas_call(functools.partial(flash_kernel, 16), out_shape=jax.ShapeDt...  6.99 us
  transfers between devices with their start and end apart: 4, of which 4 were waited for; matrix products, arithmetic and copies ran while one was open for 5% of the time, Pallas kernels for 2%

profile of v1, /device:TPU:1, one launch (start us, length us, event | category | flops | bytes accessed | tf_op | source)
XLA Modules:
  0.0 282.1 jit_solution(7648959203820779751)
XLA Ops:
  7.3 0.9 copy.20
  8.3 1.0 copy.21
  9.2 1.0 copy.22
  10.2 1.0 copy.23
  11.1 1.0 copy.24
  12.3 5.1 %all_to_all.35 = bf16[128,2,768]{0,2,1:T(8,128)(2,1)S(1)} all-to-all(bf16[128,2,768]{0,2,1:T(8,128)(2,1)S(1)} %constant_dynamic-update-slice_fusion), channel_id=1, replica_groups=mesh['z'=4,'y'=4,'core'=2,'x'=4] {'core'}, dimensions={1} | all-to-all | bytes 786432 | tf_op jit(solution)/shard_map/all_to_all | solution.py:101
  17.3 0.9 copy.25
  18.4 1.0 fusion.8
  19.4 25.3 %all-gather.7.cloned.1.call-done = bf16[512,4096]{1,0:T(8,128)(2,1)} async-done(((bf16[64,4096]{1,0:T(8,128)(2,1)}), bf16[512,4096]{1,0:T(8,128)(2,1)}) %all-gather.7.cloned.1.call-update) | async-done | bytes 4194320 | tf_op jit(solution)/shard_map/all_gather | solution.py:98
  44.7 63.0 %all-gather.5.cloned.1.call-done = bf16[4096,768]{1,0:T(8,128)(2,1)} async-done(((bf16[256,768]{1,0:T(8,128)(2,1)}), bf16[4096,768]{1,0:T(8,128)(2,1)}) %all-gather.5.cloned.1.call-update) | async-done | bytes 6291472 | tf_op jit(solution)/shard_map/all_gather | solution.py:102
  107.7 7.0 %convolution_bitcast_fusion = f32[512,768]{1,0:T(8,128)S(1)} fusion(bf16[512,4096]{1,0:T(8,128)(2,1)} %all-gather.7.cloned.1.call-done, bf16[4096,768]{1,0:T(8,128)(2,1)} %all-gather.5.cloned.1.call-done), kind=kOutput, calls=%fused_computation.1 | convolution fusion | flops 3221225472 | bytes 12058624 | tf_op jit(solution)/shard_map/dot_general | solution.py:103
  115.4 1.1 fusion.1
  116.5 0.8 pad_maximum_fusion
  118.6 69.4 %all-gather.9.cloned.1.call-done = bf16[8192,512]{1,0:T(8,128)(2,1)} async-done(((bf16[512,512]{1,0:T(8,128)(2,1)}), bf16[8192,512]{1,0:T(8,128)(2,1)}) %all-gather.9.cloned.1.call-update) | async-done | bytes 8388624 | tf_op jit(solution)/shard_map/all_gather | solution.py:107
  188.0 4.7 %slice.88.v_ref = bf16[8192,256]{1,0:T(8,128)(2,1)} slice(bf16[8192,512]{1,0:T(8,128)(2,1)} %all-gather.9.cloned.1.call-done), slice={[0:8192], [256:512]} | slice | bytes 8388608 | tf_op jit(solution)/shard_map/slice | solution.py:108
  192.8 1.4 copy-done
  194.2 2.2 fusion.9
  196.4 7.0 %shard_map.91 = bf16[512,256]{1,0:T(8,128)(2,1)} custom-call(bf16[512,128]{1,0:T(8,128)(2,1)} %get-tuple-element.11.q1_ref, bf16[512,128]{1,0:T(8,128)(2,1)} %get-tuple-element.10.q2_ref, bf16[8192,128]{1,0:T(8,128)(2,1)} %get-tuple-element.8.k1_ref, bf16[8192,128]{1,0:T(8,128)(2,1)} %get-tuple-element.7.k2_ref, bf16[8192,256]{1,0:T(8,128)(2,1)} %slice.88.v_ref, ...), custom_call_target="tpu_custom_call" | custom-call | flops 6000000000 | bytes 10000000 | tf_op jit(solution)/shard_map/pallas_call | solution.py:80
  203.4 2.9 %all_gather.18 = bf16[512,512]{1,0:T(8,128)(2,1)S(1)} all-gather(bf16[512,256]{1,0:T(8,128)(2,1)} %shard_map.91), channel_id=1, replica_groups=mesh['z'=4,'y'=4,'core'=2,'x'=4] {'core'}, dimensions={1}, use_global_device_ids=true | all-gather | bytes 786432 | tf_op jit(solution)/shard_map/all_gather | solution.py:111
  206.3 29.0 %all-gather.11.cloned.1.call-done = bf16[512,2048]{1,0:T(8,128)(2,1)} async-done(((bf16[512,128]{1,0:T(8,128)(2,1)}), bf16[512,2048]{1,0:T(8,128)(2,1)}) %all-gather.11.cloned.1.call-update) | async-done | bytes 2097168 | tf_op jit(solution)/shard_map/all_gather | solution.py:112
  235.3 2.8 %convolution_convert_fusion = bf16[512,2048]{1,0:T(8,128)(2,1)S(1)} fusion(bf16[512,512]{1,0:T(8,128)(2,1)S(1)} %all_gather.18, bf16[512,2048]{1,0:T(8,128)(2,1)} %all-gather.11.cloned.1.call-done), kind=kOutput, calls=%fused_computation | convolution fusion | flops 1074790400 | bytes 4718592 | tf_op jit(solution)/shard_map/dot_general | solution.py:113
  238.4 27.6 %all_to_all.36 = bf16[2,4,64,2048]{3,2,0,1:T(8,128)(2,1)S(1)} all-to-all(bf16[2,4,64,2048]{3,2,0,1:T(8,128)(2,1)S(1)} %copy.27), channel_id=1, replica_groups=mesh['z'=4,'y'=4,'core'=2,'x'=4] {'x'}, dimensions={1} | all-to-all | bytes 4194304 | tf_op jit(solution)/shard_map/all_to_all | solution.py:115
  266.5 7.2 %all_to_all.37 = bf16[2,64,1,2048]{3,1,2,0:T(8,128)(2,1)S(1)} all-to-all(bf16[2,64,1,2048]{3,1,2,0:T(8,128)(2,1)S(1)} %bitcast.33), channel_id=1, replica_groups=mesh['z'=4,'y'=4,'core'=2,'x'=4] {'core'}, dimensions={0} | all-to-all | bytes 1048576 | tf_op jit(solution)/shard_map/all_to_all | solution.py:117
  274.4 1.2 reshape.48
  (26 shorter events, 4.1 us)
Async XLA Ops:
  6.5 38.2 %all-gather.7.cloned.1.call-start = ((), (), s32[]{:S(2)}) async-start(), calls=%async_computation.4 | async-start | bytes 4718592 | tf_op jit(solution)/shard_map/all_gather | solution.py:98
  7.3 100.4 %all-gather.5.cloned.1.call-start = ((), (), s32[]{:S(2)}) async-start(), calls=%async_computation.3 | async-start | bytes 6684672 | tf_op jit(solution)/shard_map/all_gather | solution.py:102
  18.3 169.8 %all-gather.9.cloned.1.call-start = ((), (), s32[]{:S(2)}) async-start(), calls=%async_computation.5 | async-start | bytes 8912896 | tf_op jit(solution)/shard_map/all_gather | solution.py:107
  115.4 2.6 copy-start.1
  117.4 118.0 %all-gather.11.cloned.1.call-start = ((), (), s32[]{:S(2)}) async-start(), calls=%async_computation.6 | async-start | bytes 2228224 | tf_op jit(solution)/shard_map/all_gather | solution.py:112
  188.0 6.2 %copy-start = (bf16[8192,512]{1,0:T(8,128)(2,1)S(1)}, bf16[8192,512]{1,0:T(8,128)(2,1)}, u32[]{:S(2)}) copy-start(bf16[8192,512]{1,0:T(8,128)(2,1)} %all-gather.9.cloned.1.call-done) | copy-start | bytes 25165828
Sparse Core Ops, SparseCore 0:
  9.0 35.5 all-gather.6
  46.8 60.7 all-gather.4
  117.5 70.4 all-gather.8
  190.0 45.2 all-gather.10
